TPU v7x, 32 devices: a whole 2x2x4 slice. The times are simulated.
32 devices in a mesh: ep: 16 (over z, y, x), tp: 2 (over core).
Axes of the slice: x: 2, y: 2, z: 4, core: 2. Of those that a mesh axis runs over, the one named last changes fastest.
Arguments:
- tokens: bfloat16 [512, 2048], P('ep', 'tp')
- norm1_gain: float32 [2048], P('tp'), may hold values from 0.1 to 1.9
- w_query: bfloat16 [2048, 1024], P('tp'), may hold values from -0.125 to 0.125
- w_key: bfloat16 [2048, 128], P('tp'), may hold values from -0.125 to 0.125
- w_value: bfloat16 [2048, 128], P('tp'), may hold values from -0.125 to 0.125
- head_bias: float32 [16], P('tp'), may hold values from -7 to -1.5
- key_cache: bfloat16 [512, 1024, 128], P('ep', None, 'tp'), may hold values from -6 to 6
- value_cache: bfloat16 [512, 1024, 128], P('ep', None, 'tp'), may hold values from -6 to 6
- seq_lengths: int32 [512], P('ep'), may hold values from 1 to 1024, as said below
- w_out: bfloat16 [1024, 2048], P('tp'), may hold values from -0.375 to 0.375
- norm2_gain: float32 [2048], P('tp'), may hold values from 0.5 to 8
- route_ids: int32 [512, 4], P('ep'), may hold values from 0 to 15, all different within a row; in each aligned block of 32 rows (0 to 31, 32 to 63, ...) at most 16 rows name the same one
- route_logits: float32 [512, 4], P('ep'), may hold values from -6 to 6
- expert_gate: bfloat16 [16, 2048, 2048], P('ep', None, 'tp'), may hold values from -0.125 to 0.125
- expert_up: bfloat16 [16, 2048, 2048], P('ep', None, 'tp'), may hold values from -0.125 to 0.125
- expert_down: bfloat16 [16, 2048, 2048], P('ep', 'tp'), may hold values from -0.125 to 0.125
Outputs:
- mixed_out: bfloat16 [512, 2048], P('ep', 'tp')
- new_key: bfloat16 [512, 128], P('ep', 'tp')
- new_value: bfloat16 [512, 128], P('ep', 'tp')
Inputs may be any that keep to these rules, and one draw needn't show every extreme that they name: A sequence attends to its first seq_lengths cache positions; in every draw some sequence has exactly 1024. `route_ids`: each row names 4 different experts. Among the rows of one device no expert is named more than 16 times, and in every draw some expert is named exactly 16 times by some device's rows.
All inputs are finite; a program needn't handle non-finite values.
Results may differ from a plain program's by a relative error of at most 0.028.
Values may be sent and summed in bfloat16 or wider, within the bound.
A program may use at most 128 MiB of HBM per device.

v0:
```python
import jax
import jax.numpy as jnp
from jax import lax
from jax.sharding import PartitionSpec as P

HEAD = 64


LN_EPS = 1e-05
SWIGLU_ALPHA = 1.702
SWIGLU_LIMIT = 7.0


def heads_first(matrices, portions):
    pieces = [
        matrix.reshape(matrix.shape[0], portions, matrix.shape[1] // portions)
        for matrix in matrices
    ]
    joined = jnp.concatenate(pieces, axis=2)
    return joined.reshape(joined.shape[0], -1)


def normalize(values, total_sum, square_sum, columns, norm_gain):
    widened = values.astype(jnp.float32)
    average = total_sum / columns
    spread = square_sum / columns - average * average
    return (widened - average[:, None]) * lax.rsqrt(spread + LN_EPS)[:, None] * norm_gain


def strictly_after(count):
    rows = lax.broadcasted_iota(jnp.int32, (count, count), 0)
    cols = lax.broadcasted_iota(jnp.int32, (count, count), 1)
    return (rows > cols).astype(jnp.float32)


def later_sums(spent_log):
    positions = spent_log.shape[-1]
    block_len = 128
    blocks = positions // block_len
    lead = spent_log.shape[:-1]
    split = spent_log.reshape(lead + (blocks, block_len))
    inside = jnp.einsum(
        "...nj,js->...ns",
        split,
        strictly_after(block_len),
        precision=lax.Precision.HIGHEST,
        preferred_element_type=jnp.float32,
    )
    totals = jnp.sum(split, axis=-1)
    beyond = jnp.einsum(
        "...j,ji->...i",
        totals,
        strictly_after(blocks),
        precision=lax.Precision.HIGHEST,
        preferred_element_type=jnp.float32,
    )
    return (inside + beyond[..., None]).reshape(spent_log.shape)


def local(
    tokens,
    norm1_gain,
    w_query,
    w_key,
    w_value,
    head_bias,
    key_cache,
    value_cache,
    seq_lengths,
    w_out,
    norm2_gain,
    route_ids,
    route_logits,
    expert_gate,
    expert_up,
    expert_down,
):
    portions = lax.axis_size("tp")
    ep_count = lax.axis_size("ep")
    sequences = tokens.shape[0]
    model_width = tokens.shape[1] * portions
    widened = tokens.astype(jnp.float32)
    sums_one = lax.psum((jnp.sum(widened, axis=1), jnp.sum(widened * widened, axis=1)), "tp")
    normed = normalize(tokens, sums_one[0], sums_one[1], model_width, norm1_gain).astype(
        jnp.bfloat16
    )
    query_cols = w_query.shape[1] // portions
    key_cols = w_key.shape[1] // portions
    stacked = heads_first((w_query, w_key, w_value), portions)
    partial_value = jnp.dot(normed, stacked, preferred_element_type=jnp.float32)
    projected = lax.psum_scatter(
        partial_value.astype(jnp.bfloat16), "tp", scatter_dimension=1, tiled=True
    )
    query_rows = projected[:, :query_cols]
    new_key = projected[:, query_cols : query_cols + key_cols]
    new_value = projected[:, query_cols + key_cols :]
    positions = key_cache.shape[1]
    kv_heads = key_cols // HEAD
    grouped = query_rows.reshape(sequences, kv_heads, query_cols // key_cols, HEAD)
    key_heads = key_cache.reshape(sequences, positions, kv_heads, HEAD)
    value_heads = value_cache.reshape(sequences, positions, kv_heads, HEAD)
    scores = jnp.einsum(
        "bkgd,blkd->bkgl", grouped, key_heads, preferred_element_type=jnp.float32
    ) * HEAD ** (-0.5)
    scores = scores + head_bias.reshape(kv_heads, -1)[None, :, :, None]
    live_mask = (lax.broadcasted_iota(jnp.int32, (sequences, positions), 1) < seq_lengths[:, None])[
        :, None, None, :
    ]
    spent_log = jnp.where(live_mask, jax.nn.softplus(scores), 0.0)
    tail_sum = later_sums(spent_log)
    weights = jnp.where(live_mask, jnp.exp(jax.nn.log_sigmoid(scores) - tail_sum), 0.0).astype(
        jnp.bfloat16
    )
    attended = jnp.einsum(
        "bkgl,blkd->bkgd", weights, value_heads, preferred_element_type=jnp.float32
    )
    attended = attended.astype(jnp.bfloat16).reshape(sequences, query_cols)
    out_partial = jnp.dot(attended, w_out, preferred_element_type=jnp.float32).astype(jnp.bfloat16)
    branch = lax.psum_scatter(
        out_partial.astype(jnp.float32).astype(jnp.bfloat16), "tp", scatter_dimension=1, tiled=True
    ).astype(jnp.float32)
    residual = (tokens.astype(jnp.float32) + branch).astype(jnp.bfloat16)
    whole_rows, whole_gain = (
        lax.all_gather(residual, "tp", axis=1, tiled=True),
        lax.all_gather(norm2_gain.astype(jnp.bfloat16), "tp", axis=0, tiled=True).astype(
            norm2_gain.dtype
        ),
    )
    widened_two = whole_rows.astype(jnp.float32)
    normed_two = normalize(
        whole_rows,
        jnp.sum(widened_two, axis=1),
        jnp.sum(widened_two * widened_two, axis=1),
        model_width,
        whole_gain,
    ).astype(jnp.bfloat16)
    top_count = route_ids.shape[1]
    local_experts = expert_gate.shape[0]
    experts = ep_count * local_experts
    capacity = max(2, 2 * sequences * top_count // experts)
    flat_ids = route_ids.reshape(-1)
    route_rows = flat_ids.shape[0]
    expert_hot = (flat_ids[:, None] == lax.broadcasted_iota(jnp.int32, (1, experts), 1)).astype(
        jnp.float32
    )
    before = jnp.transpose(strictly_after(route_rows))
    earlier = jnp.dot(
        before, expert_hot, precision=lax.Precision.HIGHEST, preferred_element_type=jnp.float32
    )
    rank_in = jnp.sum(earlier * expert_hot, axis=1).astype(jnp.int32)
    targets = flat_ids * capacity + rank_in
    placing = (
        targets[:, None] == lax.broadcasted_iota(jnp.int32, (1, experts * capacity), 1)
    ).astype(jnp.bfloat16)
    sources = jnp.repeat(normed_two, top_count, axis=0)
    dispatch = jnp.einsum("rs,rd->sd", placing, sources, preferred_element_type=jnp.float32)
    dispatch = dispatch.astype(jnp.bfloat16).reshape(experts, capacity, model_width)
    arrived = lax.all_to_all(dispatch, "ep", split_axis=0, concat_axis=0, tiled=True)
    grouped_in = arrived.reshape(-1, local_experts, arrived.shape[1], arrived.shape[2])
    gate_pre = jnp.einsum(
        "secd,edf->secf", grouped_in, expert_gate, preferred_element_type=jnp.float32
    )
    up_pre = jnp.einsum("secd,edf->secf", grouped_in, expert_up, preferred_element_type=jnp.float32)
    clipped = jnp.minimum(gate_pre, SWIGLU_LIMIT)
    linear = jnp.clip(up_pre, -SWIGLU_LIMIT, SWIGLU_LIMIT)
    activated = (clipped * jax.nn.sigmoid(SWIGLU_ALPHA * clipped) * (linear + 1.0)).astype(
        jnp.bfloat16
    )
    partial_out = jnp.einsum(
        "secf,efd->secd", activated, expert_down, preferred_element_type=jnp.float32
    )
    partial_out = partial_out.astype(jnp.bfloat16)
    summed = lax.psum_scatter(
        partial_out.astype(jnp.float32).astype(jnp.bfloat16), "tp", scatter_dimension=3, tiled=True
    )
    returned = lax.all_to_all(
        summed.reshape(arrived.shape[0], arrived.shape[1], -1),
        "ep",
        split_axis=0,
        concat_axis=0,
        tiled=True,
    )
    picked = jnp.einsum(
        "rs,sd->rd",
        placing,
        returned.reshape(experts * capacity, -1),
        preferred_element_type=jnp.float32,
    )
    picked = picked.reshape(sequences, top_count, -1)
    exp_logits = jnp.exp(route_logits)
    route_probs = exp_logits / jnp.sum(exp_logits, axis=1, keepdims=True)
    moe_out = jnp.sum(route_probs[:, :, None] * picked, axis=1)
    mixed_out = (residual.astype(jnp.float32) + moe_out).astype(jnp.bfloat16)
    return (mixed_out, new_key, new_value)


def solution(mesh):
    in_specs = (
        P("ep", "tp"),
        P("tp"),
        P("tp", None),
        P("tp", None),
        P("tp", None),
        P("tp"),
        P("ep", None, "tp"),
        P("ep", None, "tp"),
        P("ep"),
        P("tp", None),
        P("tp"),
        P("ep", None),
        P("ep", None),
        P("ep", None, "tp"),
        P("ep", None, "tp"),
        P("ep", "tp", None),
    )
    out_specs = (P("ep", "tp"), P("ep", "tp"), P("ep", "tp"))
    return jax.shard_map(local, mesh=mesh, in_specs=in_specs, out_specs=out_specs, check_vma=False)
```

profile of v0, /device:TPU:0, one launch (start us, length us, event | category | flops | bytes accessed | tf_op | source)
XLA Modules:
  0.0 150.0 jit_solution(7770474083461871222)
XLA Ops:
  7.2 1.2 copy.47
  8.5 0.4 copy.49
  8.9 1.1 copy.46
  10.0 0.4 copy.48
  10.4 4.5 %reshape.200 = bf16[1024,2,512]{2,1,0:T(2,128)(2,1)} reshape(bf16[1024,1024]{1,0:T(8,128)(2,1)} %param.18) | data formatting | bytes 4194304 | tf_op jit(solution)/shard_map/reshape | solution.py:16
  14.9 5.7 %pad_maximum_fusion = bf16[1024,2,640]{2,1,0:T(2,128)(2,1)S(1)} fusion(bf16[1024,2,64]{2,1,0:T(2,128)(2,1)S(1)} %copy.49, bf16[1024,2,64]{2,1,0:T(2,128)(2,1)S(1)} %copy.48, bf16[1024,2,512]{2,1,0:T(2,128)(2,1)} %reshape.200), kind=kLoop, calls=%fused_computation.8 | loop fusion | flops 7864320 | bytes 5242880 | tf_op jit(solution)/shard_map/concatenate | solution.py:19
  20.6 2.0 %copy.62 = bf16[128,8,2,640]{3,1,2,0:T(8,128)(2,1)} copy(bf16[128,8,2,640]{3,2,1,0:T(2,128)(2,1)S(1)} %bitcast.104) | data formatting | bytes 5242880
  22.6 0.1 convert_reduce_fusion.1
  22.7 2.6 %all-reduce = (f32[32]{0:T(128)S(1)}, f32[32]{0:T(128)S(1)}) all-reduce(f32[32]{0:T(128)S(1)} %get-tuple-element.6, f32[32]{0:T(128)S(1)} %get-tuple-element.5), channel_id=1, replica_groups=mesh['ep'=16,'tp'=2] {'tp'}, use_global_device_ids=true, to_apply=%region_3.0 | all-reduce | flops 64 | bytes 512 | tf_op jit(solution)/shard_map/psum | solution.py:83
  25.4 2.3 %convolution_convert_fusion.2 = bf16[32,1280]{1,0:T(8,128)(2,1)S(1)} fusion(bf16[1024,1280]{1,0:T(8,128)(2,1)} %bitcast.103, bf16[32,1024]{1,0:T(8,128)(2,1)S(1)} %copy-done.1, f32[1024]{0:T(1024)S(1)} %copy-done.4, f32[32]{0:T(128)S(1)} %get-tuple-element.16, f32[32]{0:T(128)S(1)} %get-tuple-element.15), kind=kOutput, calls=%fused_computation.13 | convolution fusion | flops 84090880 | bytes 2773248 | tf_op jit(solution)/shard_map/dot_general | solution.py:90
  27.7 0.9 copy.56
  28.7 0.1 eq.50
  28.9 0.1 iota_compare_fusion.2
  29.0 10.1 %reduce-scatter.10.cloned.1.call-done = bf16[640,32]{1,0:T(8,128)(2,1)} async-done(((bf16[1280,32]{1,0:T(8,128)(2,1)}), bf16[640,32]{1,0:T(8,128)(2,1)}) %reduce-scatter.10.cloned.1.call-update) | async-done | bytes 40976
  39.1 0.9 slice.12
  40.0 0.1 copy.61
  40.2 2.8 %fusion.18 = f32[32,8,1024]{2,1,0:T(8,128)S(1)} fusion(bf16[32,8,64]{2,1,0:T(8,128)(2,1)S(1)} %copy.61, bf16[32,1024,64]{1,2,0:T(8,128)(2,1)} %param.22, f32[8]{0:T(128)S(1)} %copy-done.7), kind=kOutput, calls=%fused_computation.18 | convolution fusion | flops 34078720 | bytes 5275680 | tf_op jit(solution)/shard_map/bkgd,blkd->bkgl/dot_general | solution.py:102
  43.0 1.7 %fusion.85 = (f32[32,8,8]{1,2,0:T(8,128)S(1)}, f32[32,8,8,128]{3,1,2,0:T(8,128)}) fusion(f32[32,8,1024]{2,1,0:T(8,128)S(1)} %fusion.18, pred[32,1024]{1,0:T(8,128)(4,1)S(1)} %iota_compare_fusion.2), kind=kLoop, calls=%fused_computation.91 | loop fusion | flops 2095104 | bytes 2138112 | tf_op jit(solution)/shard_map/reduce_sum | solution.py:49
  44.7 0.1 copy.51
  44.9 0.1 fusion.78
  45.0 0.1 copy.52
  45.1 2.9 %convolution_add_fusion = f32[32,8,8,128]{3,2,1,0:T(8,128)} fusion(f32[32,8,8,128]{3,1,2,0:T(8,128)} %get-tuple-element.10, f32[32,8,8]{2,1,0:T(8,128)S(1)} %copy.52), kind=kOutput, calls=%fused_computation.16 | convolution fusion | flops 402931712 | bytes 2105344 | tf_op jit(solution)/shard_map/...nj,js->...ns/dot_general | solution.py:42
  48.0 2.4 %reshape.206 = f32[32,8,1024]{2,1,0:T(8,128)} reshape(f32[32,8,8,128]{3,2,1,0:T(8,128)} %convolution_add_fusion) | data formatting | bytes 2097152 | tf_op jit(solution)/shard_map/reshape | solution.py:57
  50.5 3.7 %convolution_convert_fusion.3 = bf16[32,8,64]{2,1,0:T(8,128)(2,1)S(1)} fusion(bf16[32,1024,64]{1,2,0:T(8,128)(2,1)} %param.23, f32[32,8,1024]{2,1,0:T(8,128)} %reshape.206, f32[32,8,1024]{2,1,0:T(8,128)S(1)} %fusion.18, pred[32,1024]{1,0:T(8,128)(4,1)S(1)} %iota_compare_fusion.2), kind=kOutput, calls=%fused_computation.27 | convolution fusion | flops 36454400 | bytes 6356992 | tf_op jit(solution)/shard_map/bkgl,blkd->bkgd/dot_general | solution.py:114
  54.2 0.1 reshape.207
  54.3 1.1 convolution_convert_fusion.1
  55.5 0.2 fusion.38
  55.7 1.8 %all_gather.7 = bf16[2048]{0:T(1024)(128)(2,1)S(1)} all-gather(bf16[1024]{0:T(1024)(128)(2,1)S(1)} %convert_element_type.97), channel_id=1, replica_groups=mesh['ep'=16,'tp'=2] {'tp'}, dimensions={0}, use_global_device_ids=true | all-gather | bytes 6144 | tf_op jit(solution)/shard_map/all_gather | solution.py:125
  57.5 6.8 %reduce-scatter.6.cloned.1.call-done = bf16[32,1024]{1,0:T(8,128)(2,1)} async-done(((bf16[32,2048]{1,0:T(8,128)(2,1)}), bf16[32,1024]{1,0:T(8,128)(2,1)}) %reduce-scatter.6.cloned.1.call-update) | async-done | bytes 65552 | tf_op jit(solution)/shard_map/reduce_scatter | solution.py:119
  64.3 0.9 fusion.65
  65.2 1.9 %all_gather.6 = bf16[32,2048]{1,0:T(8,128)(2,1)S(1)} all-gather(bf16[32,1024]{1,0:T(8,128)(2,1)S(1)} %fusion.65), channel_id=1, replica_groups=mesh['ep'=16,'tp'=2] {'tp'}, dimensions={1}, use_global_device_ids=true | all-gather | bytes 196608 | tf_op jit(solution)/shard_map/all_gather | solution.py:124
  67.1 0.1 convert_reduce_fusion
  67.2 0.1 fusion.59
  67.4 0.2 broadcast_in_dim.17
  67.6 0.1 reshape.208
  67.7 0.5 convolution_convert_fusion
  68.3 33.3 %all_to_all.10 = bf16[16,16,2048]{2,1,0:T(8,128)(2,1)S(1)} all-to-all(bf16[16,16,2048]{2,1,0:T(8,128)(2,1)S(1)} %bitcast.105), channel_id=1, replica_groups=mesh['ep'=16,'tp'=2] {'ep'}, dimensions={0} | all-to-all | bytes 2097152 | tf_op jit(solution)/shard_map/all_to_all | solution.py:158
  101.5 4.5 %fusion.15 = f32[16,1,16,1024]{3,2,0,1:T(8,128)} fusion(bf16[16,16,2048]{2,1,0:T(8,128)(2,1)S(1)} %all_to_all.10, bf16[1,2048,1024]{2,1,0:T(8,128)(2,1)} %param.29), kind=kOutput, calls=%fused_computation.15 | convolution fusion | flops 1074003968 | bytes 6291456 | tf_op jit(solution)/shard_map/secd,edf->secf/dot_general | solution.py:160
  106.0 7.3 %fusion.9 = bf16[16,1,16,2048]{3,2,0,1:T(8,128)(2,1)} fusion(bf16[1,1024,2048]{2,1,0:T(8,128)(2,1)} %param.31, bf16[16,16,2048]{2,1,0:T(8,128)(2,1)S(1)} %all_to_all.10, bf16[1,2048,1024]{2,1,0:T(8,128)(2,1)} %param.30, f32[16,1,16,1024]{3,2,0,1:T(8,128)} %fusion.15), kind=kOutput, calls=%fused_computation.11 | convolution fusion | flops 2150367232 | bytes 11534336 | tf_op jit(solution)/shard_map/secf,efd->secd/dot_general | solution.py:169
  113.3 7.0 %reduce-scatter.8.cloned.1.call-done = bf16[16,1,16,1024]{3,2,0,1:T(8,128)(2,1)} async-done(((bf16[16,1,16,2048]{3,2,0,1:T(8,128)(2,1)}), bf16[16,1,16,1024]{3,2,0,1:T(8,128)(2,1)}) %reduce-scatter.8.cloned.1.call-update) | async-done | bytes 524304 | tf_op jit(solution)/shard_map/reduce_scatter | solution.py:173
  120.3 6.8 %all-to-all-start.1 = ((bf16[16,16,1024]{2,1,0:T(8,128)(2,1)}), bf16[16,16,1024]{2,1,0:T(8,128)(2,1)S(1)}, u32[]{:S(2)}, u32[]{:S(2)}) async-start(bf16[16,16,1024]{2,1,0:T(8,128)(2,1)} %bitcast.109), calls=%async_computation.3 | async-start | bytes 1048576 | tf_op jit(solution)/shard_map/all_to_all | solution.py:176
  127.1 0.1 convert_element_type.95
  127.3 0.7 fusion.87
  128.0 0.7 copy.59
  128.7 0.7 copy.60
  129.4 13.1 %all-to-all-done.1 = bf16[16,16,1024]{2,1,0:T(8,128)(2,1)S(1)} async-done(((bf16[16,16,1024]{2,1,0:T(8,128)(2,1)}), bf16[16,16,1024]{2,1,0:T(8,128)(2,1)S(1)}, u32[]{:S(2)}, u32[]{:S(2)}) %all-to-all-start.1) | async-done | bytes 524320 | tf_op jit(solution)/shard_map/all_to_all | solution.py:176
  142.5 0.3 fusion.37
  142.8 0.6 add_convert_fusion
  (33 shorter events, 0.5 us)
Async XLA Ops:
  7.2 47.2 %copy-start = (bf16[512,2048]{1,0:T(8,128)(2,1)S(1)}, bf16[512,2048]{1,0:T(8,128)(2,1)}, u32[]{:S(2)}) copy-start(bf16[512,2048]{1,0:T(8,128)(2,1)} %param.25) | copy-start | bytes 6291460
  7.2 31.9 %reduce-scatter.10.cloned.1.call-start = ((), (), s32[]{:S(2)}) async-start(), calls=%async_computation.7 | async-start | bytes 491520
  14.9 7.7 %copy-start.1 = (bf16[32,1024]{1,0:T(8,128)(2,1)S(1)}, bf16[32,1024]{1,0:T(8,128)(2,1)}, u32[]{:S(2)}) copy-start(bf16[32,1024]{1,0:T(8,128)(2,1)} %param.16) | copy-start | bytes 196612
  14.9 10.5 %copy-start.4 = (f32[1024]{0:T(1024)S(1)}, f32[1024]{0:T(1024)}, u32[]{:S(2)}) copy-start(f32[1024]{0:T(1024)} %param.17) | copy-start | bytes 12292
  20.6 8.1 %copy-start.2 = (s32[32,4]{0,1:T(4,128)S(1)}, s32[32,4]{0,1:T(4,128)}, u32[]{:S(2)}) copy-start(s32[32,4]{0,1:T(4,128)} %param.27) | copy-start | bytes 1540
  20.6 8.3 %copy-start.6 = (s32[32]{0:T(128)S(1)}, s32[32]{0:T(128)}, u32[]{:S(2)}) copy-start(s32[32]{0:T(128)} %param.24) | copy-start | bytes 388
  20.6 19.6 %copy-start.7 = (f32[8]{0:T(128)S(1)}, f32[8]{0:T(128)}, u32[]{:S(2)}) copy-start(f32[8]{0:T(128)} %param.21) | copy-start | bytes 100
  28.6 35.7 %reduce-scatter.6.cloned.1.call-start = ((), (), s32[]{:S(2)}) async-start(), calls=%async_computation.5 | async-start | bytes 196608 | tf_op jit(solution)/shard_map/reduce_scatter | solution.py:119
  50.5 5.2 %copy-start.5 = (f32[1024]{0:T(1024)S(1)}, f32[1024]{0:T(1024)}, u32[]{:S(2)}) copy-start(f32[1024]{0:T(1024)} %param.26) | copy-start | bytes 12292
  55.5 64.8 %reduce-scatter.8.cloned.1.call-start = ((), (), s32[]{:S(2)}) async-start(), calls=%async_computation.6 | async-start | bytes 1572864 | tf_op jit(solution)/shard_map/reduce_scatter | solution.py:173
  106.0 21.2 %copy-start.3 = (f32[32,4]{0,1:T(4,128)S(1)}, f32[32,4]{0,1:T(4,128)}, u32[]{:S(2)}) copy-start(f32[32,4]{0,1:T(4,128)} %param.28) | copy-start | bytes 1540
  120.3 22.3 %all-to-all-start.1 = ((bf16[16,16,1024]{2,1,0:T(8,128)(2,1)}), bf16[16,16,1024]{2,1,0:T(8,128)(2,1)S(1)}, u32[]{:S(2)}, u32[]{:S(2)}) async-start(bf16[16,16,1024]{2,1,0:T(8,128)(2,1)} %bitcast.109), calls=%async_computation.3 | async-start | bytes 1048576 | tf_op jit(solution)/shard_map/all_to_all | solution.py:176
Sparse Core Ops, SparseCore 0:
  28.7 10.3 reduce-scatter.9
  55.6 8.7 reduce-scatter.5
  113.4 6.7 reduce-scatter.7
where the time goes:
time: 151 us; the launch traced here: 150 us
  blocking collectives  39.6 us (26%)
  waiting for transfers between devices  37.1 us (25%)
  matrix products  25.8 us (17%)
  local copies, waits for them, and re-layouts  17.1 us (11%)
  between operations  14 us (9%)
  other arithmetic  9.49 us (6%)
  starting transfers between devices  6.91 us (5%)
    all_to_all x1, blocking collectives, local(): lax.all_to_all(dispatch, 'ep', split_axis=0, concat_axis=0, tiled=True)  33.3 us
    all_to_all x1, waiting for transfers between devices, local(): lax.all_to_all(summed.reshape(arrived.shape[0], arrived.shape[1], -1), 'e...  13.1 us
    unnamed x4, waiting for transfers between devices  10.2 us
    dot_general x1, matrix products, local(): jnp.einsum('secf,efd->secd', activated, expert_down, preferred_element_ty...  7.26 us
    reduce_scatter x1, waiting for transfers between devices, local(): lax.psum_scatter(partial_out.astype(jnp.float32).astype(jnp.bfloat16), 't...  6.96 us
    reduce_scatter x1, waiting for transfers between devices, local(): lax.psum_scatter(out_partial.astype(jnp.float32).astype(jnp.bfloat16), 't...  6.81 us
    all_to_all x1, starting transfers between devices, local(): lax.all_to_all(summed.reshape(arrived.shape[0], arrived.shape[1], -1), 'e...  6.79 us
    unnamed x23, local copies, waits for them, and re-layouts  6.68 us
  transfers between devices with their start and end apart: 4, of which 4 were waited for; matrix products, arithmetic and copies ran while one was open for 2% of the time, Pallas kernels for 0%

commit v1 on v0

v1 whole, which is shorter than its diff:
```python
import functools

import jax
import jax.numpy as jnp
from jax import lax
from jax.experimental import pallas as pl
from jax.experimental.pallas import tpu as pltpu
from jax.sharding import PartitionSpec as P

HEAD = 64
LN_EPS = 1e-05
SWIGLU_ALPHA = 1.702
SWIGLU_LIMIT = 7.0
MESH = pl.DeviceIdType.MESH
F32 = jnp.float32
BF16 = jnp.bfloat16
DEAD = -1e30
POS_BLOCK = 256
COL_BLOCK = 256


def dot(a, b):
    return jnp.dot(a, b, preferred_element_type=F32)


def kernel(
    n,
    cap,
    tok_hbm,
    g1_hbm,
    wq_hbm,
    wk_hbm,
    wv_hbm,
    bias_ref,
    kc_hbm,
    vc_hbm,
    lens_ref,
    wo_hbm,
    g2_hbm,
    ids_hbm,
    logits_hbm,
    gate_hbm,
    up_hbm,
    down_hbm,
    out_ref,
    nk_ref,
    nv_ref,
    x_own,
    x_peer,
    g1,
    wq,
    wk,
    wv,
    kc,
    vc,
    wo,
    g2,
    ids,
    logits,
    gate,
    up,
    down,
    proj_send,
    proj_recv,
    q_rows,
    z_ref,
    att_ref,
    part_send,
    part_recv,
    res_ref,
    disp,
    recv_own,
    recv_peer,
    gate_acc,
    up_acc,
    act_ref,
    down_send,
    down_recv,
    down_own,
    back_send,
    back_recv,
    comb_ref,
    load_sem,
    one_send,
    one_recv,
    disp_send_sem,
    disp_recv_sem,
    fwd_send_sem,
    fwd_recv_sem,
    down_send_sem,
    down_recv_sem,
    back_send_sem,
    back_recv_sem,
    local_sem,
):
    ep = lax.axis_index("ep")
    tp = lax.axis_index("tp")
    other = 1 - tp
    seqs, half = x_own.shape
    width = 2 * half
    slots = n * cap

    loads = []
    pairs = (
        (tok_hbm, x_own),
        (g1_hbm, g1),
        (wq_hbm, wq),
        (wk_hbm, wk),
        (wv_hbm, wv),
        (kc_hbm, kc),
        (vc_hbm, vc),
        (wo_hbm, wo),
        (g2_hbm, g2),
        (ids_hbm, ids),
        (logits_hbm, logits),
        (gate_hbm, gate),
        (up_hbm, up),
        (down_hbm, down),
    )
    for i, (src, dst) in enumerate(pairs):
        copy = pltpu.make_async_copy(src, dst, load_sem.at[i])
        copy.start()
        loads.append(copy)

    def peer_copy(src, dst, i):
        return pltpu.make_async_remote_copy(
            src_ref=src,
            dst_ref=dst,
            send_sem=one_send.at[i],
            recv_sem=one_recv.at[i],
            device_id=(ep, other),
            device_id_type=MESH,
        )

    barrier = pltpu.get_barrier_semaphore()
    pl.semaphore_signal(barrier, inc=1, device_id=(ep, other), device_id_type=MESH)

    def greet(i, carry):
        pl.semaphore_signal(
            barrier, inc=1, device_id=(lax.rem(ep + i, n), tp), device_id_type=MESH
        )
        return carry

    lax.fori_loop(1, n, greet, 0)
    pl.semaphore_wait(barrier, n)

    loads[0].wait()
    tok_copy = peer_copy(x_own, x_peer, 0)
    tok_copy.start()
    loads[1].wait()
    for i in (2, 3, 4):
        loads[i].wait()
    mine = x_own[...].astype(F32)
    tok_copy.wait()
    theirs = x_peer[...].astype(F32)

    def stats(a, b):
        total = jnp.sum(a, axis=1, keepdims=True) + jnp.sum(b, axis=1, keepdims=True)
        square = jnp.sum(a * a, axis=1, keepdims=True) + jnp.sum(b * b, axis=1, keepdims=True)
        mean = total / width
        return mean, lax.rsqrt(square / width - mean * mean + LN_EPS)

    mean, scale = stats(mine, theirs)
    normed = ((mine - mean) * scale * g1[...]).astype(BF16)
    pq = dot(normed, wq[...])
    pk = dot(normed, wk[...])
    pv = dot(normed, wv[...])
    qc = pq.shape[1] // 2
    kcols = pk.shape[1] // 2
    first = tp == 0
    proj_send[:, :qc] = jnp.where(first, pq[:, qc:], pq[:, :qc])
    proj_send[:, qc : qc + kcols] = jnp.where(first, pk[:, kcols:], pk[:, :kcols])
    proj_send[:, qc + kcols :] = jnp.where(first, pv[:, kcols:], pv[:, :kcols])
    proj_copy = peer_copy(proj_send, proj_recv, 1)
    proj_copy.start()

    loads[9].wait()
    loads[10].wait()
    top = ids.shape[0]
    slot_row = lax.broadcasted_iota(jnp.int32, (slots, seqs), 0)
    slot_expert = slot_row // cap
    slot_rank = slot_row - slot_expert * cap
    id_rows = ids[...]
    raw = jnp.exp(logits[...])
    probs = raw / jnp.sum(raw, axis=0, keepdims=True)
    hot = jnp.zeros((slots, seqs), F32)
    prob_hot = jnp.zeros((slots, seqs), F32)
    for k in range(top):
        match = id_rows[k : k + 1, :] == slot_expert
        hot = hot + jnp.where(match, 1.0, 0.0)
        prob_hot = prob_hot + jnp.where(match, probs[k : k + 1, :], 0.0)
    earlier = (
        lax.broadcasted_iota(jnp.int32, (seqs, seqs), 0)
        < lax.broadcasted_iota(jnp.int32, (seqs, seqs), 1)
    )
    rank = dot(hot.astype(BF16), jnp.where(earlier, 1.0, 0.0).astype(BF16))
    chosen = (hot > 0.5) & (jnp.abs(rank - slot_rank.astype(F32)) < 0.5)
    placing = jnp.where(chosen, 1.0, 0.0).astype(BF16)
    weight = jnp.where(chosen, prob_hot, 0.0)
    weight_hi = weight.astype(BF16)
    weight_lo = (weight - weight_hi.astype(F32)).astype(BF16)
    comb_ref[0] = weight_hi
    comb_ref[1] = weight_lo

    groups = qc // HEAD
    bias = jnp.zeros((groups, 1), F32)
    head_row = lax.broadcasted_iota(jnp.int32, (groups, 1), 0)
    for h in range(groups):
        bias = bias + jnp.where(head_row == h, bias_ref[h], 0.0)

    own_q = jnp.where(first, pq[:, :qc], pq[:, qc:])
    own_k = jnp.where(first, pk[:, :kcols], pk[:, kcols:])
    own_v = jnp.where(first, pv[:, :kcols], pv[:, kcols:])
    proj_copy.wait()
    query = (own_q + proj_recv[:, :qc]).astype(BF16).astype(F32)
    nk_ref[...] = (own_k + proj_recv[:, qc : qc + kcols]).astype(BF16)
    nv_ref[...] = (own_v + proj_recv[:, qc + kcols :]).astype(BF16)
    for h in range(groups):
        q_rows[:, h, :] = query[:, h * HEAD : (h + 1) * HEAD]

    positions = kc.shape[2]
    loads[5].wait()
    place = lax.broadcasted_iota(jnp.int32, (groups, positions), 1)

    def score_step(i, carry):
        for j in range(4):
            b = i * 4 + j
            s = dot(q_rows[b].astype(BF16), kc[b]) * HEAD ** (-0.5) + bias
            z_ref[pl.ds(pl.multiple_of(b * groups, groups), groups), :] = jnp.where(
                place < lens_ref[b], s, DEAD
            )
        return carry

    lax.fori_loop(0, seqs // 4, score_step, 0)

    after = (
        lax.broadcasted_iota(jnp.int32, (POS_BLOCK, POS_BLOCK), 0)
        > lax.broadcasted_iota(jnp.int32, (POS_BLOCK, POS_BLOCK), 1)
    )
    after = jnp.where(after, 1.0, 0.0).astype(BF16)
    row_block = 64

    def break_step(i, carry):
        rows = pl.ds(pl.multiple_of(i * row_block, row_block), row_block)
        beyond = jnp.zeros((row_block, 1), F32)
        for c in reversed(range(positions // POS_BLOCK)):
            cols = slice(c * POS_BLOCK, (c + 1) * POS_BLOCK)
            z = z_ref[rows, cols]
            tail = jnp.log1p(jnp.exp(-jnp.abs(z)))
            spent = jnp.maximum(z, 0.0) + tail
            hi = spent.astype(BF16)
            lo = (spent - hi.astype(F32)).astype(BF16)
            sums = dot(jnp.concatenate([hi, lo], axis=0), after)
            inside = sums[:row_block] + sums[row_block:]
            z_ref[rows, cols] = jnp.exp(jnp.minimum(z, 0.0) - tail - (inside + beyond))
            beyond = beyond + inside[:, :1] + spent[:, :1]
        return carry

    lax.fori_loop(0, seqs * groups // row_block, break_step, 0)

    loads[6].wait()

    def read_step(i, carry):
        rows = pl.ds(pl.multiple_of(i * 4 * groups, 4 * groups), 4 * groups)
        weights = z_ref[rows, :].astype(BF16)
        values = vc[pl.ds(i * 4, 4)].reshape(4 * HEAD, positions)
        mixed = lax.dot_general(
            weights, values, (((1,), (1,)), ((), ())), preferred_element_type=F32
        )
        for j in range(4):
            att_ref[i * 4 + j] = mixed[
                j * groups : (j + 1) * groups, j * HEAD : (j + 1) * HEAD
            ]
        return carry

    lax.fori_loop(0, seqs // 4, read_step, 0)
    attended = jnp.concatenate([att_ref[:, h, :] for h in range(groups)], axis=1).astype(BF16)

    loads[7].wait()
    part = dot(attended, wo[...]).astype(BF16)
    part_send[0] = part[:, :half]
    part_send[1] = part[:, half:]
    part_copy = peer_copy(part_send, part_recv, 2)
    part_copy.start()
    loads[8].wait()
    part_copy.wait()
    mine = x_own[...].astype(F32)
    theirs = x_peer[...].astype(F32)
    res_own = (mine + (part_send[tp].astype(F32) + part_recv[tp].astype(F32))).astype(BF16)
    res_other = (
        theirs + (part_send[other].astype(F32) + part_recv[other].astype(F32))
    ).astype(BF16)
    res_ref[...] = res_own
    mine = res_own.astype(F32)
    mean, scale = stats(mine, res_other.astype(F32))
    normed_two = ((mine - mean) * scale * g2[...]).astype(BF16)
    disp[...] = dot(placing, normed_two).astype(BF16).reshape(n, cap, half)

    def disp_copy(i):
        to = lax.rem(ep + i, n)
        return pltpu.make_async_remote_copy(
            src_ref=disp.at[to],
            dst_ref=recv_own.at[ep],
            send_sem=disp_send_sem.at[i],
            recv_sem=disp_recv_sem.at[i],
            device_id=(to, tp),
            device_id_type=MESH,
        )

    def disp_arrival(i):
        source = lax.rem(ep + n - i, n)
        return pltpu.make_async_remote_copy(
            src_ref=disp.at[source],
            dst_ref=recv_own.at[source],
            send_sem=disp_send_sem.at[i],
            recv_sem=disp_recv_sem.at[i],
            device_id=(source, tp),
            device_id_type=MESH,
        )

    def fwd_copy(i):
        source = lax.rem(ep + n - i, n)
        return pltpu.make_async_remote_copy(
            src_ref=recv_own.at[source],
            dst_ref=recv_peer.at[source],
            send_sem=fwd_send_sem.at[i],
            recv_sem=fwd_recv_sem.at[i],
            device_id=(ep, other),
            device_id_type=MESH,
        )

    def start_disp(i, carry):
        disp_copy(i).start()
        return carry

    lax.fori_loop(1, n, start_disp, 0)
    keep = pltpu.make_async_copy(disp.at[ep], recv_own.at[ep], local_sem.at[0])
    keep.start()
    keep.wait()
    fwd_copy(0).start()

    def pass_on(i, carry):
        disp_arrival(i).wait_recv()
        fwd_copy(i).start()
        return carry

    lax.fori_loop(1, n, pass_on, 0)

    loads[11].wait()
    loads[12].wait()
    rows_block = min(slots, 256)
    row_blocks = slots // rows_block
    per_block = rows_block // cap
    hidden = gate.shape[1]

    def first_half(i, carry):
        cols = pl.ds(pl.multiple_of(i * COL_BLOCK, COL_BLOCK), COL_BLOCK)
        depth = pl.ds(pl.multiple_of(tp * half, half), half)
        for r in range(row_blocks):
            rows = recv_own[r * per_block : (r + 1) * per_block].reshape(rows_block, half)
            at = slice(r * rows_block, (r + 1) * rows_block)
            gate_acc[at, cols] = dot(rows, gate[depth, cols])
            up_acc[at, cols] = dot(rows, up[depth, cols])
        return carry

    lax.fori_loop(0, hidden // COL_BLOCK, first_half, 0)

    def finish_fwd(i, carry):
        fwd_copy(i).wait()
        return carry

    lax.fori_loop(0, n, finish_fwd, 0)

    def second_half(i, carry):
        cols = pl.ds(pl.multiple_of(i * COL_BLOCK, COL_BLOCK), COL_BLOCK)
        depth = pl.ds(pl.multiple_of(other * half, half), half)
        for r in range(row_blocks):
            rows = recv_peer[r * per_block : (r + 1) * per_block].reshape(rows_block, half)
            at = slice(r * rows_block, (r + 1) * rows_block)
            g = gate_acc[at, cols] + dot(rows, gate[depth, cols])
            u = up_acc[at, cols] + dot(rows, up[depth, cols])
            c = jnp.minimum(g, SWIGLU_LIMIT)
            linear = jnp.clip(u, -SWIGLU_LIMIT, SWIGLU_LIMIT)
            act_ref[at, cols] = (
                c * jax.nn.sigmoid(SWIGLU_ALPHA * c) * (linear + 1.0)
            ).astype(BF16)
        return carry

    lax.fori_loop(0, hidden // COL_BLOCK, second_half, 0)

    loads[13].wait()
    tiles = half // COL_BLOCK

    def down_copy(i):
        return pltpu.make_async_remote_copy(
            src_ref=down_send.at[i],
            dst_ref=down_recv.at[i],
            send_sem=down_send_sem.at[i],
            recv_sem=down_recv_sem.at[i],
            device_id=(ep, other),
            device_id_type=MESH,
        )

    def down_tile(ref, side, i):
        cols = pl.ds(pl.multiple_of(side * half + i * COL_BLOCK, COL_BLOCK), COL_BLOCK)
        for r in range(row_blocks):
            at = slice(r * rows_block, (r + 1) * rows_block)
            ref[i, at, :] = dot(act_ref[at, :], down[:, cols]).astype(BF16)

    def down_other(i, carry):
        down_tile(down_send, other, i)
        down_copy(i).start()
        return carry

    lax.fori_loop(0, tiles, down_other, 0)

    def down_mine(i, carry):
        down_tile(down_own, tp, i)
        return carry

    lax.fori_loop(0, tiles, down_mine, 0)
    for i in range(tiles):
        down_copy(i).wait()
        total = (down_own[i].astype(F32) + down_recv[i].astype(F32)).astype(BF16)
        back_send[:, :, i * COL_BLOCK : (i + 1) * COL_BLOCK] = total.reshape(n, cap, COL_BLOCK)

    def back_copy(i):
        to = lax.rem(ep + i, n)
        return pltpu.make_async_remote_copy(
            src_ref=back_send.at[to],
            dst_ref=back_recv.at[ep],
            send_sem=back_send_sem.at[i],
            recv_sem=back_recv_sem.at[i],
            device_id=(to, tp),
            device_id_type=MESH,
        )

    def back_arrival(i):
        source = lax.rem(ep + n - i, n)
        return pltpu.make_async_remote_copy(
            src_ref=back_send.at[source],
            dst_ref=back_recv.at[source],
            send_sem=back_send_sem.at[i],
            recv_sem=back_recv_sem.at[i],
            device_id=(source, tp),
            device_id_type=MESH,
        )

    def start_back(i, carry):
        back_copy(i).start()
        return carry

    lax.fori_loop(1, n, start_back, 0)
    keep = pltpu.make_async_copy(back_send.at[ep], back_recv.at[ep], local_sem.at[1])
    keep.start()
    keep.wait()

    def finish_back(i, carry):
        back_arrival(i).wait_recv()
        return carry

    lax.fori_loop(1, n, finish_back, 0)

    back = back_recv[...].reshape(slots, half)
    over_slots = (((0,), (0,)), ((), ()))
    moe = lax.dot_general(comb_ref[0], back, over_slots, preferred_element_type=F32)
    moe = moe + lax.dot_general(comb_ref[1], back, over_slots, preferred_element_type=F32)
    out_ref[...] = (res_ref[...].astype(F32) + moe).astype(BF16)

    def finish_sends(i, carry):
        disp_copy(i).wait_send()
        back_copy(i).wait_send()
        return carry

    lax.fori_loop(1, n, finish_sends, 0)


def local(
    tokens,
    norm1_gain,
    w_query,
    w_key,
    w_value,
    head_bias,
    key_cache,
    value_cache,
    seq_lengths,
    w_out,
    norm2_gain,
    route_ids,
    route_logits,
    expert_gate,
    expert_up,
    expert_down,
):
    n = lax.axis_size("ep")
    seqs, half = tokens.shape
    top = route_ids.shape[1]
    experts = n * expert_gate.shape[0]
    capacity = max(2, 2 * seqs * top // experts)
    cap = -(-capacity // 16) * 16
    slots = n * cap
    qc = w_query.shape[1] // 2
    kcols = w_key.shape[1] // 2
    groups = qc // HEAD
    positions = key_cache.shape[1]
    hidden = expert_gate.shape[2]
    tiles = half // COL_BLOCK
    keys = jnp.swapaxes(key_cache, 1, 2)
    values = jnp.swapaxes(value_cache, 1, 2)
    operands = (
        tokens,
        norm1_gain.reshape(1, -1),
        w_query,
        w_key,
        w_value,
        head_bias,
        keys,
        values,
        seq_lengths,
        w_out,
        norm2_gain.reshape(1, -1),
        route_ids.T,
        route_logits.T,
        expert_gate.reshape(expert_gate.shape[1:]),
        expert_up.reshape(expert_up.shape[1:]),
        expert_down.reshape(expert_down.shape[1:]),
    )
    in_smem = (5, 8)
    in_specs = [
        pl.BlockSpec(memory_space=pltpu.SMEM if i in in_smem else pl.ANY)
        for i in range(len(operands))
    ]
    vmem = pl.BlockSpec(memory_space=pltpu.VMEM)
    loaded = [
        pltpu.VMEM(a.shape, a.dtype) for i, a in enumerate(operands) if i not in in_smem
    ]
    dma = pltpu.SemaphoreType.DMA
    scratch = (
        [loaded[0], loaded[0]]
        + loaded[1:]
        + [
            pltpu.VMEM((seqs, qc + 2 * kcols), F32),
            pltpu.VMEM((seqs, qc + 2 * kcols), F32),
            pltpu.VMEM((seqs, groups, HEAD), F32),
            pltpu.VMEM((seqs * groups, positions), F32),
            pltpu.VMEM((seqs, groups, HEAD), F32),
            pltpu.VMEM((2, seqs, half), BF16),
            pltpu.VMEM((2, seqs, half), BF16),
            pltpu.VMEM((seqs, half), BF16),
            pltpu.VMEM((n, cap, half), BF16),
            pltpu.VMEM((n, cap, half), BF16),
            pltpu.VMEM((n, cap, half), BF16),
            pltpu.VMEM((slots, hidden), F32),
            pltpu.VMEM((slots, hidden), F32),
            pltpu.VMEM((slots, hidden), BF16),
            pltpu.VMEM((tiles, slots, COL_BLOCK), BF16),
            pltpu.VMEM((tiles, slots, COL_BLOCK), BF16),
            pltpu.VMEM((tiles, slots, COL_BLOCK), BF16),
            pltpu.VMEM((n, cap, half), BF16),
            pltpu.VMEM((n, cap, half), BF16),
            pltpu.VMEM((2, slots, seqs), BF16),
            dma((len(loaded),)),
            dma((3,)),
            dma((3,)),
            dma((n,)),
            dma((n,)),
            dma((n,)),
            dma((n,)),
            dma((tiles,)),
            dma((tiles,)),
            dma((n,)),
            dma((n,)),
            dma((2,)),
        ]
    )
    return pl.pallas_call(
        functools.partial(kernel, n, cap),
        out_shape=(
            jax.ShapeDtypeStruct((seqs, half), BF16),
            jax.ShapeDtypeStruct((seqs, kcols), BF16),
            jax.ShapeDtypeStruct((seqs, kcols), BF16),
        ),
        in_specs=in_specs,
        out_specs=(vmem, vmem, vmem),
        scratch_shapes=scratch,
        compiler_params=pltpu.CompilerParams(
            collective_id=0, has_side_effects=True, vmem_limit_bytes=64 * 1024 * 1024 - 65536
        ),
    )(*operands)


def solution(mesh):
    in_specs = (
        P("ep", "tp"),
        P("tp"),
        P("tp", None),
        P("tp", None),
        P("tp", None),
        P("tp"),
        P("ep", None, "tp"),
        P("ep", None, "tp"),
        P("ep"),
        P("tp", None),
        P("tp"),
        P("ep", None),
        P("ep", None),
        P("ep", None, "tp"),
        P("ep", None, "tp"),
        P("ep", "tp", None),
    )
    out_specs = (P("ep", "tp"), P("ep", "tp"), P("ep", "tp"))
    return jax.shard_map(local, mesh=mesh, in_specs=in_specs, out_specs=out_specs, check_vma=False)
```

time: 151 us -> 55.7 us (0.37)
  the two profiles are of different devices: /device:TPU:0 before, /device:TPU:28 now
where the time goes in v1:
time: 55.7 us; the launch traced here: 55.4 us
  Pallas kernels  50.7 us (91%)
  local copies, waits for them, and re-layouts  4.06 us (7%)
  between operations  0.65 us (1%)
    pallas_call x1, Pallas kernels, local(): pl.pallas_call(functools.partial(kernel, n, cap), out_shape=(jax.ShapeDty...  50.7 us
    unnamed x3, local copies, waits for them, and re-layouts  4.06 us

profile of v1, /device:TPU:28, one launch (start us, length us, event | category | flops | bytes accessed | tf_op | source)
XLA Modules:
  0.0 55.4 jit_solution(18353461199574452923)
XLA Ops:
  0.6 50.7 %shard_map.175 = (bf16[32,1024]{1,0:T(8,128)(2,1)}, bf16[32,64]{1,0:T(8,128)(2,1)}, bf16[32,64]{1,0:T(8,128)(2,1)}) custom-call(bf16[32,1024]{1,0:T(8,128)(2,1)} %tok_hbm.1, f32[1,1024]{1,0:T(1,128)} %bitcast.14, bf16[1024,1024]{1,0:T(8,128)(2,1)} %wq_hbm.1, bf16[1024,128]{1,0:T(8,128)(2,1)} %wk_hbm.1, bf16[1024,128]{1,0:T(8,128)(2,1)} %wv_hbm.1, ...), custom_call_target="tpu_custom_call" | custom-call | tf_op jit(solution)/shard_map/pallas_call | solution.py:577
  51.4 1.5 %copy.22 = bf16[32,1024]{1,0:T(8,128)(2,1)} copy(bf16[32,1024]{1,0:T(8,128)(2,1)} %get-tuple-element.6) | data formatting | bytes 131072
  52.8 1.3 %copy.23 = bf16[32,64]{1,0:T(8,128)(2,1)} copy(bf16[32,64]{1,0:T(8,128)(2,1)} %get-tuple-element.7) | data formatting | bytes 8192
  54.1 1.3 %copy.24 = bf16[32,64]{1,0:T(8,128)(2,1)} copy(bf16[32,64]{1,0:T(8,128)(2,1)} %get-tuple-element.8) | data formatting | bytes 8192

commit v2 on v1

--- a/solution.py
+++ b/solution.py
@@ -68,6 +68,10 @@
     part_send,
     part_recv,
     res_ref,
+    tables_send,
+    tables_recv,
+    rows_ref,
+    rows_recv,
     disp,
     recv_own,
     recv_peer,
@@ -79,10 +83,17 @@
     down_own,
     back_send,
     back_recv,
-    comb_ref,
+    sum_send,
+    sum_recv,
     load_sem,
     one_send,
     one_recv,
+    table_send_sem,
+    table_recv_sem,
+    rows_send_sem,
+    rows_recv_sem,
+    sum_send_sem,
+    sum_recv_sem,
     disp_send_sem,
     disp_recv_sem,
     fwd_send_sem,
@@ -119,8 +130,9 @@
     )
     for i, (src, dst) in enumerate(pairs):
         copy = pltpu.make_async_copy(src, dst, load_sem.at[i])
-        copy.start()
         loads.append(copy)
+    for i in (0, 2, 3, 4, 1, 9, 10, 8):
+        loads[i].start()
 
     def peer_copy(src, dst, i):
         return pltpu.make_async_remote_copy(
@@ -135,14 +147,28 @@
     barrier = pltpu.get_barrier_semaphore()
     pl.semaphore_signal(barrier, inc=1, device_id=(ep, other), device_id_type=MESH)
 
-    def greet(i, carry):
-        pl.semaphore_signal(
-            barrier, inc=1, device_id=(lax.rem(ep + i, n), tp), device_id_type=MESH
-        )
-        return carry
-
-    lax.fori_loop(1, n, greet, 0)
-    pl.semaphore_wait(barrier, n)
+    planes = tables_send.shape[0]
+    plane = n // planes
+    level = ep // plane
+    spot = ep % plane
+
+    def column(i):
+        return lax.rem(level + i, planes) * plane + spot
+
+    def beside(i):
+        return level * plane + lax.rem(spot + i, plane)
+
+    def greet_column(i, carry):
+        pl.semaphore_signal(barrier, inc=1, device_id=(column(i), tp), device_id_type=MESH)
+        return carry
+
+    def greet_beside(i, carry):
+        pl.semaphore_signal(barrier, inc=1, device_id=(beside(i), tp), device_id_type=MESH)
+        return carry
+
+    lax.fori_loop(1, planes, greet_column, 0)
+    lax.fori_loop(1, plane, greet_beside, 0)
+    pl.semaphore_wait(barrier, planes + plane - 1)
 
     loads[0].wait()
     tok_copy = peer_copy(x_own, x_peer, 0)
@@ -150,6 +176,8 @@
     loads[1].wait()
     for i in (2, 3, 4):
         loads[i].wait()
+    for i in (5, 6, 7):
+        loads[i].start()
     mine = x_own[...].astype(F32)
     tok_copy.wait()
     theirs = x_peer[...].astype(F32)
@@ -174,6 +202,8 @@
     proj_copy = peer_copy(proj_send, proj_recv, 1)
     proj_copy.start()
 
+    for i in (11, 12, 13):
+        loads[i].start()
     loads[9].wait()
     loads[10].wait()
     top = ids.shape[0]
@@ -199,8 +229,12 @@
     weight = jnp.where(chosen, prob_hot, 0.0)
     weight_hi = weight.astype(BF16)
     weight_lo = (weight - weight_hi.astype(F32)).astype(BF16)
-    comb_ref[0] = weight_hi
-    comb_ref[1] = weight_lo
+    group = plane * cap
+    for q in range(planes):
+        at = slice(q * group, (q + 1) * group)
+        tables_send[q, 0] = placing[at]
+        tables_send[q, 1] = weight_hi[at]
+        tables_send[q, 2] = weight_lo[at]
 
     groups = qc // HEAD
     bias = jnp.zeros((groups, 1), F32)
@@ -217,6 +251,33 @@
     nv_ref[...] = (own_v + proj_recv[:, qc + kcols :]).astype(BF16)
     for h in range(groups):
         q_rows[:, h, :] = query[:, h * HEAD : (h + 1) * HEAD]
+
+    def to_column(src, dst, sends, recvs, i):
+        to = lax.rem(level + i, planes)
+        return pltpu.make_async_remote_copy(
+            src_ref=src.at[to],
+            dst_ref=dst.at[level],
+            send_sem=sends.at[i],
+            recv_sem=recvs.at[i],
+            device_id=(column(i), tp),
+            device_id_type=MESH,
+        )
+
+    def from_column(src, dst, sends, recvs, i):
+        source = lax.rem(level + planes - i, planes)
+        return pltpu.make_async_remote_copy(
+            src_ref=src.at[source],
+            dst_ref=dst.at[source],
+            send_sem=sends.at[i],
+            recv_sem=recvs.at[i],
+            device_id=(source * plane + spot, tp),
+            device_id_type=MESH,
+        )
+
+    table_args = (tables_send, tables_recv, table_send_sem, table_recv_sem)
+    for i in range(1, planes):
+        to_column(*table_args, i).start()
+    tables_recv[level] = tables_send[level]
 
     positions = kc.shape[2]
     loads[5].wait()
@@ -294,63 +355,100 @@
     mine = res_own.astype(F32)
     mean, scale = stats(mine, res_other.astype(F32))
     normed_two = ((mine - mean) * scale * g2[...]).astype(BF16)
-    disp[...] = dot(placing, normed_two).astype(BF16).reshape(n, cap, half)
-
-    def disp_copy(i):
-        to = lax.rem(ep + i, n)
-        return pltpu.make_async_remote_copy(
-            src_ref=disp.at[to],
-            dst_ref=recv_own.at[ep],
-            send_sem=disp_send_sem.at[i],
-            recv_sem=disp_recv_sem.at[i],
-            device_id=(to, tp),
-            device_id_type=MESH,
-        )
-
-    def disp_arrival(i):
-        source = lax.rem(ep + n - i, n)
-        return pltpu.make_async_remote_copy(
-            src_ref=disp.at[source],
-            dst_ref=recv_own.at[source],
-            send_sem=disp_send_sem.at[i],
-            recv_sem=disp_recv_sem.at[i],
-            device_id=(source, tp),
-            device_id_type=MESH,
-        )
-
-    def fwd_copy(i):
-        source = lax.rem(ep + n - i, n)
-        return pltpu.make_async_remote_copy(
-            src_ref=recv_own.at[source],
-            dst_ref=recv_peer.at[source],
-            send_sem=fwd_send_sem.at[i],
-            recv_sem=fwd_recv_sem.at[i],
+    rows_ref[...] = normed_two
+
+    def rows_copy(i):
+        return pltpu.make_async_remote_copy(
+            src_ref=rows_ref,
+            dst_ref=rows_recv.at[level],
+            send_sem=rows_send_sem.at[i],
+            recv_sem=rows_recv_sem.at[i],
+            device_id=(column(i), tp),
+            device_id_type=MESH,
+        )
+
+    def rows_arrival(i):
+        source = lax.rem(level + planes - i, planes)
+        return pltpu.make_async_remote_copy(
+            src_ref=rows_ref,
+            dst_ref=rows_recv.at[source],
+            send_sem=rows_send_sem.at[i],
+            recv_sem=rows_recv_sem.at[i],
+            device_id=(source * plane + spot, tp),
+            device_id_type=MESH,
+        )
+
+    def beside_copy(src, dst, sends, recvs, i, j):
+        source = lax.rem(level + planes - i, planes)
+        to = lax.rem(spot + j, plane)
+        return pltpu.make_async_remote_copy(
+            src_ref=src.at[source, to],
+            dst_ref=dst.at[source, spot],
+            send_sem=sends.at[i, j],
+            recv_sem=recvs.at[i, j],
+            device_id=(level * plane + to, tp),
+            device_id_type=MESH,
+        )
+
+    def beside_arrival(src, dst, sends, recvs, i, j):
+        source = lax.rem(level + planes - i, planes)
+        giver = lax.rem(spot + plane - j, plane)
+        return pltpu.make_async_remote_copy(
+            src_ref=src.at[source, giver],
+            dst_ref=dst.at[source, giver],
+            send_sem=sends.at[i, j],
+            recv_sem=recvs.at[i, j],
+            device_id=(level * plane + giver, tp),
+            device_id_type=MESH,
+        )
+
+    def fwd_copy(i, j):
+        source = lax.rem(level + planes - i, planes)
+        giver = lax.rem(spot + plane - j, plane)
+        return pltpu.make_async_remote_copy(
+            src_ref=recv_own.at[source, giver],
+            dst_ref=recv_peer.at[source, giver],
+            send_sem=fwd_send_sem.at[i, j],
+            recv_sem=fwd_recv_sem.at[i, j],
             device_id=(ep, other),
             device_id_type=MESH,
         )
 
-    def start_disp(i, carry):
-        disp_copy(i).start()
-        return carry
-
-    lax.fori_loop(1, n, start_disp, 0)
-    keep = pltpu.make_async_copy(disp.at[ep], recv_own.at[ep], local_sem.at[0])
-    keep.start()
-    keep.wait()
-    fwd_copy(0).start()
-
-    def pass_on(i, carry):
-        disp_arrival(i).wait_recv()
-        fwd_copy(i).start()
-        return carry
-
-    lax.fori_loop(1, n, pass_on, 0)
+    disp_args = (disp, recv_own, disp_send_sem, disp_recv_sem)
+    for i in range(1, planes):
+        rows_copy(i).start()
+    for i in range(1, planes):
+        from_column(*table_args, i).wait_recv()
+    keeps = []
+
+    def place_rows(i, rows):
+        source = lax.rem(level + planes - i, planes)
+        placed = dot(tables_recv[source, 0], rows).astype(BF16)
+        disp[source] = placed.reshape(plane, cap, half)
+        for j in range(1, plane):
+            beside_copy(*disp_args, i, j).start()
+        keep = pltpu.make_async_copy(
+            disp.at[source, spot], recv_own.at[source, spot], local_sem.at[i]
+        )
+        keep.start()
+        keeps.append(keep)
+
+    place_rows(0, normed_two)
+    for i in range(1, planes):
+        rows_arrival(i).wait_recv()
+        place_rows(i, rows_recv[lax.rem(level + planes - i, planes)])
+    for i in range(planes):
+        keeps[i].wait()
+        fwd_copy(i, 0).start()
+        for j in range(1, plane):
+            beside_arrival(*disp_args, i, j).wait_recv()
+            fwd_copy(i, j).start()
 
     loads[11].wait()
     loads[12].wait()
     rows_block = min(slots, 256)
     row_blocks = slots // rows_block
-    per_block = rows_block // cap
+    per_block = rows_block // group
     hidden = gate.shape[1]
 
     def first_half(i, carry):
@@ -365,11 +463,9 @@
 
     lax.fori_loop(0, hidden // COL_BLOCK, first_half, 0)
 
-    def finish_fwd(i, carry):
-        fwd_copy(i).wait()
-        return carry
-
-    lax.fori_loop(0, n, finish_fwd, 0)
+    for i in range(planes):
+        for j in range(plane):
+            fwd_copy(i, j).wait()
 
     def second_half(i, carry):
         cols = pl.ds(pl.multiple_of(i * COL_BLOCK, COL_BLOCK), COL_BLOCK)
@@ -422,57 +518,73 @@
     for i in range(tiles):
         down_copy(i).wait()
         total = (down_own[i].astype(F32) + down_recv[i].astype(F32)).astype(BF16)
-        back_send[:, :, i * COL_BLOCK : (i + 1) * COL_BLOCK] = total.reshape(n, cap, COL_BLOCK)
-
-    def back_copy(i):
-        to = lax.rem(ep + i, n)
-        return pltpu.make_async_remote_copy(
-            src_ref=back_send.at[to],
-            dst_ref=back_recv.at[ep],
-            send_sem=back_send_sem.at[i],
-            recv_sem=back_recv_sem.at[i],
-            device_id=(to, tp),
-            device_id_type=MESH,
-        )
-
-    def back_arrival(i):
-        source = lax.rem(ep + n - i, n)
-        return pltpu.make_async_remote_copy(
-            src_ref=back_send.at[source],
-            dst_ref=back_recv.at[source],
-            send_sem=back_send_sem.at[i],
-            recv_sem=back_recv_sem.at[i],
-            device_id=(source, tp),
-            device_id_type=MESH,
-        )
-
-    def start_back(i, carry):
-        back_copy(i).start()
-        return carry
-
-    lax.fori_loop(1, n, start_back, 0)
-    keep = pltpu.make_async_copy(back_send.at[ep], back_recv.at[ep], local_sem.at[1])
-    keep.start()
-    keep.wait()
-
-    def finish_back(i, carry):
-        back_arrival(i).wait_recv()
-        return carry
-
-    lax.fori_loop(1, n, finish_back, 0)
-
-    back = back_recv[...].reshape(slots, half)
+        back_send[:, :, :, i * COL_BLOCK : (i + 1) * COL_BLOCK] = total.reshape(
+            planes, plane, cap, COL_BLOCK
+        )
+
+    back_args = (back_send, back_recv, back_send_sem, back_recv_sem)
+    order = tuple(range(1, planes)) + (0,)
+    back_keeps = {}
+    for i in order:
+        for j in range(1, plane):
+            beside_copy(*back_args, i, j).start()
+        source = lax.rem(level + planes - i, planes)
+        back_keeps[i] = pltpu.make_async_copy(
+            back_send.at[source, spot], back_recv.at[source, spot], local_sem.at[planes + i]
+        )
+        back_keeps[i].start()
+
+    def sum_copy(i):
+        source = lax.rem(level + planes - i, planes)
+        return pltpu.make_async_remote_copy(
+            src_ref=sum_send.at[source],
+            dst_ref=sum_recv.at[level],
+            send_sem=sum_send_sem.at[i],
+            recv_sem=sum_recv_sem.at[i],
+            device_id=(source * plane + spot, tp),
+            device_id_type=MESH,
+        )
+
+    def sum_arrival(i):
+        giver = lax.rem(level + i, planes)
+        return pltpu.make_async_remote_copy(
+            src_ref=sum_send.at[giver],
+            dst_ref=sum_recv.at[giver],
+            send_sem=sum_send_sem.at[i],
+            recv_sem=sum_recv_sem.at[i],
+            device_id=(giver * plane + spot, tp),
+            device_id_type=MESH,
+        )
+
     over_slots = (((0,), (0,)), ((), ()))
-    moe = lax.dot_general(comb_ref[0], back, over_slots, preferred_element_type=F32)
-    moe = moe + lax.dot_general(comb_ref[1], back, over_slots, preferred_element_type=F32)
-    out_ref[...] = (res_ref[...].astype(F32) + moe).astype(BF16)
-
-    def finish_sends(i, carry):
-        disp_copy(i).wait_send()
-        back_copy(i).wait_send()
-        return carry
-
-    lax.fori_loop(1, n, finish_sends, 0)
+    total = res_ref[...].astype(F32)
+    for i in order:
+        source = lax.rem(level + planes - i, planes)
+        back_keeps[i].wait()
+        for j in range(1, plane):
+            beside_arrival(*back_args, i, j).wait_recv()
+        back = back_recv[source].reshape(group, half)
+        mixed = lax.dot_general(
+            tables_recv[source, 1], back, over_slots, preferred_element_type=F32
+        ) + lax.dot_general(tables_recv[source, 2], back, over_slots, preferred_element_type=F32)
+        if i == 0:
+            total = total + mixed
+        else:
+            sum_send[source] = mixed.astype(BF16)
+            sum_copy(i).start()
+    for i in range(1, planes):
+        sum_arrival(i).wait_recv()
+        total = total + sum_recv[lax.rem(level + i, planes)].astype(F32)
+    out_ref[...] = total.astype(BF16)
+
+    for i in range(1, planes):
+        to_column(*table_args, i).wait_send()
+        rows_copy(i).wait_send()
+        sum_copy(i).wait_send()
+    for i in range(planes):
+        for j in range(1, plane):
+            beside_copy(*disp_args, i, j).wait_send()
+            beside_copy(*back_args, i, j).wait_send()
 
 
 def local(
@@ -500,6 +612,8 @@
     capacity = max(2, 2 * seqs * top // experts)
     cap = -(-capacity // 16) * 16
     slots = n * cap
+    planes = 4 if n % 4 == 0 else 1
+    plane = n // planes
     qc = w_query.shape[1] // 2
     kcols = w_key.shape[1] // 2
     groups = qc // HEAD
@@ -548,30 +662,41 @@
             pltpu.VMEM((2, seqs, half), BF16),
             pltpu.VMEM((2, seqs, half), BF16),
             pltpu.VMEM((seqs, half), BF16),
-            pltpu.VMEM((n, cap, half), BF16),
-            pltpu.VMEM((n, cap, half), BF16),
-            pltpu.VMEM((n, cap, half), BF16),
+            pltpu.VMEM((planes, 3, plane * cap, seqs), BF16),
+            pltpu.VMEM((planes, 3, plane * cap, seqs), BF16),
+            pltpu.VMEM((seqs, half), BF16),
+            pltpu.VMEM((planes, seqs, half), BF16),
+            pltpu.VMEM((planes, plane, cap, half), BF16),
+            pltpu.VMEM((planes, plane, cap, half), BF16),
+            pltpu.VMEM((planes, plane, cap, half), BF16),
             pltpu.VMEM((slots, hidden), F32),
             pltpu.VMEM((slots, hidden), F32),
             pltpu.VMEM((slots, hidden), BF16),
             pltpu.VMEM((tiles, slots, COL_BLOCK), BF16),
             pltpu.VMEM((tiles, slots, COL_BLOCK), BF16),
             pltpu.VMEM((tiles, slots, COL_BLOCK), BF16),
-            pltpu.VMEM((n, cap, half), BF16),
-            pltpu.VMEM((n, cap, half), BF16),
-            pltpu.VMEM((2, slots, seqs), BF16),
+            pltpu.VMEM((planes, plane, cap, half), BF16),
+            pltpu.VMEM((planes, plane, cap, half), BF16),
+            pltpu.VMEM((planes, seqs, half), BF16),
+            pltpu.VMEM((planes, seqs, half), BF16),
             dma((len(loaded),)),
             dma((3,)),
             dma((3,)),
-            dma((n,)),
-            dma((n,)),
-            dma((n,)),
-            dma((n,)),
+            dma((planes,)),
+            dma((planes,)),
+            dma((planes,)),
+            dma((planes,)),
+            dma((planes,)),
+            dma((planes,)),
+            dma((planes, plane)),
+            dma((planes, plane)),
+            dma((planes, plane)),
+            dma((planes, plane)),
             dma((tiles,)),
             dma((tiles,)),
-            dma((n,)),
-            dma((n,)),
-            dma((2,)),
+            dma((planes, plane)),
+            dma((planes, plane)),
+            dma((2 * planes,)),
         ]
     )
     return pl.pallas_call(

time: 55.7 us -> 54.3 us (0.975)
  the two profiles are of different devices: /device:TPU:28 before, /device:TPU:0 now
where the time goes in v2:
time: 54.3 us; the launch traced here: 54 us
  Pallas kernels  49.3 us (91%)
  local copies, waits for them, and re-layouts  4.06 us (7%)
  between operations  0.65 us (1%)
    pallas_call x1, Pallas kernels, local(): pl.pallas_call(functools.partial(kernel, n, cap), out_shape=(jax.ShapeDty...  49.3 us
    unnamed x3, local copies, waits for them, and re-layouts  4.06 us

profile of v2, /device:TPU:0, one launch (start us, length us, event | category | flops | bytes accessed | tf_op | source)
XLA Modules:
  0.0 54.0 jit_solution(753963440305049235)
XLA Ops:
  0.6 49.3 %shard_map.175 = (bf16[32,1024]{1,0:T(8,128)(2,1)}, bf16[32,64]{1,0:T(8,128)(2,1)}, bf16[32,64]{1,0:T(8,128)(2,1)}) custom-call(bf16[32,1024]{1,0:T(8,128)(2,1)} %tok_hbm.1, f32[1,1024]{1,0:T(1,128)} %bitcast.14, bf16[1024,1024]{1,0:T(8,128)(2,1)} %wq_hbm.1, bf16[1024,128]{1,0:T(8,128)(2,1)} %wk_hbm.1, bf16[1024,128]{1,0:T(8,128)(2,1)} %wv_hbm.1, ...), custom_call_target="tpu_custom_call" | custom-call | tf_op jit(solution)/shard_map/pallas_call | solution.py:702
  49.9 1.5 %copy.22 = bf16[32,1024]{1,0:T(8,128)(2,1)} copy(bf16[32,1024]{1,0:T(8,128)(2,1)} %get-tuple-element.6) | data formatting | bytes 131072
  51.4 1.3 %copy.23 = bf16[32,64]{1,0:T(8,128)(2,1)} copy(bf16[32,64]{1,0:T(8,128)(2,1)} %get-tuple-element.7) | data formatting | bytes 8192
  52.7 1.3 %copy.24 = bf16[32,64]{1,0:T(8,128)(2,1)} copy(bf16[32,64]{1,0:T(8,128)(2,1)} %get-tuple-element.8) | data formatting | bytes 8192
